TPU v7x, 32 devices: a whole 2x2x4 slice. The times are simulated.
32 devices in a mesh: ep: 16 (over z, y, x), tp: 2 (over core).
Axes of the slice: x: 2, y: 2, z: 4, core: 2. Of those that a mesh axis runs over, the one named last changes fastest.
Arguments:
- tokens: bfloat16 [1024, 1024], P('ep', 'tp'), may hold values from -6 to 6
- norm_gain: float32 [1024], P('tp'), may hold values from 0.1 to 1.9
- routing: int32 [1024, 2], P('ep'), may hold values from 0 to 31, as said below
- route_weight: float32 [1024, 2], P('ep'), may hold values from 0.25 to 1
- w_gate: bfloat16 [32, 1024, 512], P('ep', None, 'tp'), may hold values from -0.1875 to 0.1875
- w_up: bfloat16 [32, 1024, 512], P('ep', None, 'tp'), may hold values from -0.1875 to 0.1875
- w_down: bfloat16 [32, 512, 1024], P('ep', None, 'tp'), may hold values from -0.25 to 0.25
Outputs:
- mixed: bfloat16 [1024, 1024], P('ep', 'tp')
Inputs may be any that keep to these rules, and one draw needn't show every extreme that they name: `routing`: each row names 2 different experts, all in the same group of 8 consecutive expert numbers. Among the rows of one device (aligned blocks of 64 rows) no expert is named more than 8 times, and in every block some expert is named exactly 8 times.
All inputs are finite; a program needn't handle non-finite values.
Results may differ from a plain program's by a relative error of at most 0.0015.
Values may be sent and summed in bfloat16 or wider, within the bound.
A program may use at most 64 MiB of HBM per device.

v0:
```python
import jax
import jax.numpy as jnp
from jax import lax
from jax.sharding import PartitionSpec as P

CAP = 8


epsilon = 1e-06


def taken_in(shard, axis, dim, update, carry):
    whole = jax.tree.map(lambda part: lax.all_gather(part, axis, axis=dim, tiled=True), shard)
    return update(carry, whole, jnp.int32(0))


def for_sending(shard):
    def short(part):
        return part.astype(jnp.bfloat16) if part.dtype == jnp.float32 else part

    return jax.tree.map(short, shard)


def expert_rows(arrivals, gate_weight, up_weight, down_weight):
    row_total = arrivals.shape[0]
    hidden_half = gate_weight.shape[1]
    half_width = down_weight.shape[1]
    zero_acc = jnp.zeros((row_total, hidden_half), jnp.float32)

    def add_feature(totals, block_part, offset):
        span = block_part.shape[1]
        gate_rows = lax.dynamic_slice_in_dim(gate_weight, offset, span, 0)
        up_rows = lax.dynamic_slice_in_dim(up_weight, offset, span, 0)
        return (
            totals[0] + jnp.dot(block_part, gate_rows, preferred_element_type=jnp.float32),
            totals[1] + jnp.dot(block_part, up_rows, preferred_element_type=jnp.float32),
        )

    gate_acc, up_acc = taken_in(arrivals, "tp", 1, add_feature, (zero_acc, zero_acc))
    hidden = (jax.nn.silu(gate_acc) * up_acc).astype(jnp.bfloat16)

    def add_hidden(totals, block_part, offset):
        down_rows = lax.dynamic_slice_in_dim(down_weight, offset, block_part.shape[1], 0)
        return totals + jnp.dot(block_part, down_rows, preferred_element_type=jnp.float32)

    result = taken_in(hidden, "tp", 1, add_hidden, jnp.zeros((row_total, half_width), jnp.float32))
    return result.astype(jnp.bfloat16)


def local(tokens, norm_gain, routing, route_weight, w_gate, w_up, w_down):
    tok_rows, half_width = tokens.shape
    float_rows = tokens.astype(jnp.float32)
    square_sum = jnp.sum(float_rows * float_rows, axis=1)
    total_squares = lax.psum(square_sum, "tp")
    full_width = half_width * lax.axis_size("tp")
    scale = lax.rsqrt(total_squares[:, None] / full_width + epsilon)
    normed = (float_rows * scale * norm_gain[None, :]).astype(jnp.bfloat16)
    peer_count = lax.axis_size("ep")
    local_experts = w_gate.shape[0]
    experts = local_experts * peer_count
    pick_count = routing.shape[1]
    flat_expert = routing.reshape(-1).astype(jnp.int32)
    onehot = (flat_expert[:, None] == jnp.arange(experts, dtype=jnp.int32)[None, :]).astype(
        jnp.int32
    )
    earlier = jnp.cumsum(onehot, axis=0).astype(jnp.int32) - onehot
    slot_index = jnp.sum(earlier * onehot, axis=1).astype(jnp.int32)
    target = flat_expert * CAP + slot_index
    source_rows = jnp.repeat(normed, pick_count, axis=0)
    outgoing = jnp.zeros((experts * CAP, half_width), jnp.bfloat16).at[target].set(source_rows)
    outgoing = outgoing.reshape(peer_count, local_experts, CAP, half_width)
    arrived = lax.all_to_all(outgoing, "ep", split_axis=0, concat_axis=0, tiled=True)
    finished = []
    for local_index in range(local_experts):
        arrivals = arrived[:, local_index].reshape(peer_count * CAP, half_width)
        result = expert_rows(arrivals, w_gate[local_index], w_up[local_index], w_down[local_index])
        finished.append(result.reshape(peer_count, CAP, half_width))
    stacked = jnp.stack(finished, axis=1)
    returned = lax.all_to_all(
        for_sending(stacked), "ep", split_axis=0, concat_axis=0, tiled=True
    ).astype(stacked.dtype)
    returned_rows = returned.reshape(experts * CAP, half_width)
    gathered = returned_rows[target].astype(jnp.float32) * route_weight.reshape(-1)[:, None]
    combined = jnp.sum(gathered.reshape(tok_rows, pick_count, half_width), axis=1)
    return combined.astype(jnp.bfloat16)


def solution(mesh):
    in_specs = (
        P("ep", "tp"),
        P("tp"),
        P("ep", None),
        P("ep", None),
        P("ep", None, "tp"),
        P("ep", None, "tp"),
        P("ep", None, "tp"),
    )
    out_specs = P("ep", "tp")
    return jax.shard_map(local, mesh=mesh, in_specs=in_specs, out_specs=out_specs, check_vma=False)
```

profile of v0, /device:TPU:0, one launch (start us, length us, event | category | flops | bytes accessed | tf_op | source)
XLA Modules:
  0.0 51.4 jit_solution(10007299614687021656)
XLA Ops:
  0.0 0.0 copy-start.3
  0.0 0.8 %copy.17 = s32[64,2]{1,0:T(8,128)S(1)} copy(s32[64,2]{0,1:T(2,128)} %param.9) | data formatting | bytes 1024 | tf_op args[2]
  0.8 0.0 copy-done.3
  0.9 0.1 eq.15
  1.0 0.1 fusion.23
  1.1 0.2 reduce_window_sum.11
  1.3 0.0 copy-start.2
  1.3 0.2 select_reduce_fusion
  1.4 0.1 copy.16
  1.5 0.1 mul.62
  1.7 0.4 copy-done.2
  2.1 0.1 fusion.18
  2.2 0.0 copy-start.4
  2.2 2.7 %psum.7 = f32[64]{0:T(128)S(1)} all-reduce(f32[64]{0:T(128)S(1)} %fusion.18), channel_id=1, replica_groups=mesh['ep'=16,'tp'=2] {'tp'}, use_global_device_ids=true, to_apply=%region_3.4 | all-reduce | flops 64 | bytes 512 | tf_op jit(solution)/shard_map/psum | solution.py:54
  4.9 0.0 copy-done.4
  4.9 0.1 fusion.20
  5.0 0.0 copy-start
  5.0 0.1 broadcast_in_dim.5
  5.1 0.1 reshape.70
  5.1 1.1 %scatter_custom_fusion = bf16[256,512]{1,0:T(8,128)(2,1)S(1)} fusion(s32[128]{0:T(128)S(1)} %fusion.24, bf16[128,512]{1,0:T(8,128)(2,1)S(1)} %reshape.70, bf16[]{:T(256)} %constant.8.clone.1), kind=kCustom, calls=%fused_computation.33 | custom fusion | bytes 262146 | tf_op jit(solution)/shard_map/scatter | solution.py:70
  6.3 18.2 %all_to_all.10 = bf16[16,2,8,512]{3,2,1,0:T(8,128)(2,1)S(1)} all-to-all(bf16[16,2,8,512]{3,2,1,0:T(8,128)(2,1)S(1)} %bitcast.45), channel_id=1, replica_groups=mesh['ep'=16,'tp'=2] {'ep'}, dimensions={0} | all-to-all | bytes 524288 | tf_op jit(solution)/shard_map/all_to_all | solution.py:72
  24.5 0.0 copy-start.6
  24.5 2.1 %all_gather.12 = bf16[128,1024]{1,0:T(8,128)(2,1)S(1)} all-gather(bf16[128,512]{1,0:T(8,128)(2,1)S(1)} %get-tuple-element.5), channel_id=1, replica_groups=mesh['ep'=16,'tp'=2] {'tp'}, dimensions={1}, use_global_device_ids=true | all-gather | bytes 393216 | tf_op jit(solution)/shard_map/all_gather | solution.py:13
  26.6 0.0 copy-done
  26.6 0.2 fusion.10
  26.8 0.0 copy-done.6
  26.9 0.2 fusion.2
  27.1 1.9 %all_gather.13 = bf16[128,512]{1,0:T(8,128)(2,1)S(1)} all-gather(bf16[128,256]{1,0:T(8,128)(2,1)S(1)} %fusion.2), channel_id=1, replica_groups=mesh['ep'=16,'tp'=2] {'tp'}, dimensions={1}, use_global_device_ids=true | all-gather | bytes 196608 | tf_op jit(solution)/shard_map/all_gather | solution.py:13
  29.0 2.0 %all_gather.14 = bf16[128,1024]{1,0:T(8,128)(2,1)S(1)} all-gather(bf16[128,512]{1,0:T(8,128)(2,1)S(1)} %get-tuple-element.6), channel_id=1, replica_groups=mesh['ep'=16,'tp'=2] {'tp'}, dimensions={1}, use_global_device_ids=true | all-gather | bytes 393216 | tf_op jit(solution)/shard_map/all_gather | solution.py:13
  31.0 0.2 fusion.6
  31.2 0.0 copy-start.1
  31.2 0.2 fusion.3
  31.5 2.0 %all_gather.15 = bf16[128,512]{1,0:T(8,128)(2,1)S(1)} all-gather(bf16[128,256]{1,0:T(8,128)(2,1)S(1)} %fusion.3), channel_id=1, replica_groups=mesh['ep'=16,'tp'=2] {'tp'}, dimensions={1}, use_global_device_ids=true | all-gather | bytes 196608 | tf_op jit(solution)/shard_map/all_gather | solution.py:13
  33.5 0.0 copy-done.1
  33.5 0.2 fusion
  33.8 0.2 fusion.1
  34.0 0.7 %pad_maximum_fusion = bf16[16,2,8,512]{3,2,1,0:T(8,128)(2,1)} fusion(bf16[16,1,8,512]{3,2,1,0:T(8,128)(2,1)S(1)} %fusion.1, bf16[16,1,8,512]{3,2,1,0:T(8,128)(2,1)S(1)} %fusion), kind=kLoop, calls=%fused_computation.24 | loop fusion | flops 131072 | bytes 524288 | tf_op jit(solution)/shard_map/stack | solution.py:78
  34.7 0.0 copy-start.5
  34.7 4.4 %all-to-all-start.1 = ((bf16[16,2,8,512]{3,2,1,0:T(8,128)(2,1)}), bf16[16,2,8,512]{3,2,1,0:T(8,128)(2,1)S(1)}, u32[]{:S(2)}, u32[]{:S(2)}) async-start(bf16[16,2,8,512]{3,2,1,0:T(8,128)(2,1)} %pad_maximum_fusion), calls=%async_computation.1 | async-start | bytes 524288 | tf_op jit(solution)/shard_map/all_to_all | solution.py:79
  39.2 0.0 copy-done.5
  39.2 0.1 copy.20
  39.3 10.0 %all-to-all-done.1 = bf16[16,2,8,512]{3,2,1,0:T(8,128)(2,1)S(1)} async-done(((bf16[16,2,8,512]{3,2,1,0:T(8,128)(2,1)}), bf16[16,2,8,512]{3,2,1,0:T(8,128)(2,1)S(1)}, u32[]{:S(2)}, u32[]{:S(2)}) %all-to-all-start.1) | async-done | bytes 262176 | tf_op jit(solution)/shard_map/all_to_all | solution.py:79
  49.3 0.8 %gather_fusion = bf16[128,512]{1,0:T(8,128)(2,1)S(1)} fusion(bf16[256,512]{1,0:T(8,128)(2,1)S(1)} %bitcast.44, s32[1024]{0:T(1024)S(1)} %pad_clamp_fusion), kind=kCustom, calls=%fused_computation | custom fusion | bytes 262656 | tf_op jit(solution)/shard_map/gather | solution.py:83
  50.2 0.2 reshape.57
  50.3 1.0 %multiply_reduce_fusion = bf16[64,512]{1,0:T(8,128)(2,1)} fusion(f32[64,2,512]{2,1,0:T(2,128)S(1)} %reshape.57, f32[64,2]{1,0:T(8,128)S(1)} %copy.20), kind=kLoop, calls=%fused_computation.25 | loop fusion | flops 98304 | bytes 328192 | tf_op jit(solution)/shard_map/reduce_sum | solution.py:84
  (5 shorter events, 0.0 us)
Async XLA Ops:
  0.0 0.8 %copy-start.3 = (s32[64,2]{0,1:T(2,128)S(1)}, s32[64,2]{0,1:T(2,128)}, u32[]{:S(2)}) copy-start(s32[64,2]{0,1:T(2,128)} %param.9) | copy-start | bytes 1540
  1.3 0.8 %copy-start.2 = (bf16[64,512]{1,0:T(8,128)(2,1)S(1)}, bf16[64,512]{1,0:T(8,128)(2,1)}, u32[]{:S(2)}) copy-start(bf16[64,512]{1,0:T(8,128)(2,1)} %param.7) | copy-start | bytes 196612
  2.2 2.7 %copy-start.4 = (f32[512]{0:T(512)S(1)}, f32[512]{0:T(512)}, u32[]{:S(2)}) copy-start(f32[512]{0:T(512)} %param.8) | copy-start | bytes 6148
  5.0 21.6 %copy-start = (bf16[2,1024,256]{2,1,0:T(8,128)(2,1)S(1)}, bf16[2,1024,256]{2,1,0:T(8,128)(2,1)}, u32[]{:S(2)}) copy-start(bf16[2,1024,256]{2,1,0:T(8,128)(2,1)} %param.11) | copy-start | bytes 3145732
  24.5 2.4 %copy-start.6 = (bf16[2,1024,256]{2,1,0:T(8,128)(2,1)S(1)}, bf16[2,1024,256]{2,1,0:T(8,128)(2,1)}, u32[]{:S(2)}) copy-start(bf16[2,1024,256]{2,1,0:T(8,128)(2,1)} %param.12) | copy-start | bytes 3145732
  31.2 2.3 %copy-start.1 = (bf16[2,512,512]{2,1,0:T(8,128)(2,1)S(1)}, bf16[2,512,512]{2,1,0:T(8,128)(2,1)}, u32[]{:S(2)}) copy-start(bf16[2,512,512]{2,1,0:T(8,128)(2,1)} %param.13) | copy-start | bytes 3145732
  34.7 4.5 %copy-start.5 = (f32[64,2]{0,1:T(2,128)S(1)}, f32[64,2]{0,1:T(2,128)}, u32[]{:S(2)}) copy-start(f32[64,2]{0,1:T(2,128)} %param.10) | copy-start | bytes 1540
  34.7 14.6 %all-to-all-start.1 = ((bf16[16,2,8,512]{3,2,1,0:T(8,128)(2,1)}), bf16[16,2,8,512]{3,2,1,0:T(8,128)(2,1)S(1)}, u32[]{:S(2)}, u32[]{:S(2)}) async-start(bf16[16,2,8,512]{3,2,1,0:T(8,128)(2,1)} %pad_maximum_fusion), calls=%async_computation.1 | async-start | bytes 524288 | tf_op jit(solution)/shard_map/all_to_all | solution.py:79
where the time goes:
time: 51.7 us; the launch traced here: 51.4 us
  blocking collectives  28.9 us (56%)
  waiting for transfers between devices  10 us (19%)
  starting transfers between devices  4.44 us (9%)
  local copies, waits for them, and re-layouts  4.06 us (8%)
  other arithmetic  2.39 us (5%)
  matrix products  1.4 us (3%)
    all_to_all x1, blocking collectives, local(): lax.all_to_all(outgoing, 'ep', split_axis=0, concat_axis=0, tiled=True)  18.2 us
    all_to_all x1, waiting for transfers between devices, local(): lax.all_to_all(for_sending(stacked), 'ep', split_axis=0, concat_axis=0, t...  10 us
    all_gather x4, blocking collectives, taken_in(): lax.all_gather(part, axis, axis=dim, tiled=True)  8.05 us
    all_to_all x1, starting transfers between devices, local(): lax.all_to_all(for_sending(stacked), 'ep', split_axis=0, concat_axis=0, t...  4.44 us
    psum x1, blocking collectives, local(): total_squares = lax.psum(square_sum, 'tp')  2.65 us
    unnamed x16, local copies, waits for them, and re-layouts  1.38 us
    scatter x1, local copies, waits for them, and re-layouts, local(): jnp.zeros((experts * CAP, half_width), jnp.bfloat16).at[target]  1.13 us
  transfers between devices with their start and end apart: 1, of which 1 were waited for; matrix products, arithmetic and copies ran while one was open for 0% of the time, Pallas kernels for 0%

commit v1 on v0

v1 whole, which is shorter than its diff:
```python
import functools

import jax
import jax.numpy as jnp
from jax import lax
from jax.experimental import pallas as pl
from jax.experimental.pallas import tpu as pltpu
from jax.sharding import PartitionSpec as P

CAP = 8
EPSILON = 1e-06
MESH = pl.DeviceIdType.MESH


def each(count, body):
    if count <= 16:
        for k in range(1, count):
            body(k)
    else:
        lax.fori_loop(1, count, lambda k, c: (body(k), c)[1], 0)


def kernel(
    n, tok_ref, gain_ref, routing_ref, weight_ref, wg_hbm, wu_hbm, wd_hbm, out_ref,
    gains, wg, wu, wd, send_x, recv_x, send_y, recv_y,
    own_sem, far_send, far_recv, sx_sem, rx_sem, sy_sem, ry_sem,
):
    me, core = lax.axis_index("ep"), lax.axis_index("tp")
    other = 1 - core
    tokens, half = tok_ref.shape
    slots = 2 * n * CAP

    stores = ((wg_hbm, wg), (wu_hbm, wu), (wd_hbm, wd))
    own = [
        pltpu.make_async_copy(src.at[core], dst.at[core], own_sem.at[i])
        for i, (src, dst) in enumerate(stores)
    ]
    for copy in own:
        copy.start()

    barrier = pltpu.get_barrier_semaphore()

    def greet(k):
        peer = lax.rem(me + k, n)
        for c in range(2):
            pl.semaphore_signal(barrier, inc=1, device_id=(peer, c), device_id_type=MESH)

    pl.semaphore_signal(barrier, inc=1, device_id=(me, other), device_id_type=MESH)
    each(n, greet)

    gains[core] = gain_ref[...]
    experts = 2 * n
    names = lax.broadcasted_iota(jnp.int32, (tokens, experts), 1)
    picks = [routing_ref[:, k:k + 1] for k in range(2)]
    hot = [(picks[k] == names).astype(jnp.float32) for k in range(2)]
    row = lax.broadcasted_iota(jnp.int32, (tokens, tokens), 0)
    col = lax.broadcasted_iota(jnp.int32, (tokens, tokens), 1)
    before = (col < row).astype(jnp.bfloat16)
    earlier = jnp.dot(before, (hot[0] + hot[1]).astype(jnp.bfloat16), preferred_element_type=jnp.float32)
    places = lax.broadcasted_iota(jnp.int32, (tokens, slots), 1)
    chosen = []
    for k in range(2):
        rank = jnp.sum(earlier * hot[k], axis=1, keepdims=True).astype(jnp.int32)
        chosen.append(places == picks[k] * CAP + rank)
    spread = (chosen[0] | chosen[1]).astype(jnp.float32).astype(jnp.bfloat16)
    outgoing = lax.dot_general(
        spread, tok_ref[...], (((0,), (0,)), ((), ())), preferred_element_type=jnp.float32
    )
    send_x[...] = outgoing.reshape(2 * n, CAP, half).astype(jnp.bfloat16)

    pl.semaphore_wait(barrier, 2 * n - 1)

    def remote(src, dst, send, recv, peer, c):
        return pltpu.make_async_remote_copy(
            src_ref=src, dst_ref=dst, send_sem=send, recv_sem=recv,
            device_id=(peer, c), device_id_type=MESH,
        )

    def post(k):
        peer = lax.rem(me + k, n)
        for c in range(2):
            remote(send_x.at[peer * 2 + c], recv_x.at[core * n + me], sx_sem, rx_sem, peer, c).start()

    each(n, post)
    remote(send_x.at[me * 2 + other], recv_x.at[core * n + me], sx_sem, rx_sem, me, other).start()
    pltpu.make_async_copy(send_x.at[me * 2 + core], recv_x.at[core * n + me], rx_sem).start()
    far = [remote(gain_ref, gains.at[core], far_send.at[3], far_recv.at[3], me, other)] + [
        remote(src.at[other], dst.at[core], far_send.at[i], far_recv.at[i], me, other)
        for i, (src, dst) in enumerate(stores)
    ]
    for copy in far:
        copy.start()

    for copy in own:
        copy.wait()
    for copy in far:
        copy.wait()
    pltpu.make_async_copy(recv_x, recv_x, rx_sem).wait()

    rows = n * CAP
    parts = [recv_x[h * n:(h + 1) * n].astype(jnp.float32).reshape(rows, half) for h in range(2)]
    squares = sum(jnp.sum(p * p, axis=1, keepdims=True) for p in parts)
    scale = lax.rsqrt(squares / (2 * half) + EPSILON)
    normed = jnp.concatenate(
        [(p * scale * gains[h]).astype(jnp.bfloat16) for h, p in enumerate(parts)], axis=1
    )
    hidden = []
    for h in range(2):
        gate = jnp.dot(normed, wg[h], preferred_element_type=jnp.float32)
        up = jnp.dot(normed, wu[h], preferred_element_type=jnp.float32)
        hidden.append((jax.nn.silu(gate) * up).astype(jnp.bfloat16))
    hidden = jnp.concatenate(hidden, axis=1)
    for f in range(2):
        result = jnp.dot(hidden, wd[f], preferred_element_type=jnp.float32)
        send_y[f * n:(f + 1) * n] = result.reshape(n, CAP, half).astype(jnp.bfloat16)

    def reply(k):
        peer = lax.rem(me + k, n)
        for c in range(2):
            remote(send_y.at[c * n + peer], recv_y.at[me * 2 + core], sy_sem, ry_sem, peer, c).start()

    each(n, reply)
    remote(send_y.at[other * n + me], recv_y.at[me * 2 + core], sy_sem, ry_sem, me, other).start()
    pltpu.make_async_copy(send_y.at[core * n + me], recv_y.at[me * 2 + core], ry_sem).start()
    pltpu.make_async_copy(recv_y, recv_y, ry_sem).wait()

    back = recv_y[...].astype(jnp.float32).reshape(slots, half).astype(jnp.bfloat16)
    total = 0.0
    for k in range(2):
        pick = chosen[k].astype(jnp.float32).astype(jnp.bfloat16)
        total = total + weight_ref[:, k:k + 1] * jnp.dot(pick, back, preferred_element_type=jnp.float32)
    out_ref[...] = total.astype(jnp.bfloat16)
    sent = pl.ds(0, 2 * n - 1)
    pltpu.make_async_copy(send_x.at[sent], send_x.at[sent], sx_sem).wait()
    pltpu.make_async_copy(send_y.at[sent], send_y.at[sent], sy_sem).wait()


def solution(mesh):
    n = mesh.shape["ep"]

    def local(tokens, norm_gain, routing, route_weight, w_gate, w_up, w_down):
        rows, half = tokens.shape
        assert w_gate.shape[0] == 2 and mesh.shape["tp"] == 2
        vmem = pl.BlockSpec(memory_space=pltpu.VMEM)
        far = pl.BlockSpec(memory_space=pl.ANY)
        blocks = pltpu.VMEM((2 * n, CAP, half), jnp.bfloat16)
        dma = pltpu.SemaphoreType.DMA
        return pl.pallas_call(
            functools.partial(kernel, n),
            out_shape=jax.ShapeDtypeStruct((rows, half), jnp.bfloat16),
            in_specs=[vmem] * 4 + [far] * 3,
            out_specs=vmem,
            scratch_shapes=[
                pltpu.VMEM((2, 1, half), jnp.float32),
                pltpu.VMEM(w_gate.shape, jnp.bfloat16),
                pltpu.VMEM(w_up.shape, jnp.bfloat16),
                pltpu.VMEM(w_down.shape, jnp.bfloat16),
                blocks, blocks, blocks, blocks,
                dma((3,)), dma((4,)), dma((4,)), dma, dma, dma, dma,
            ],
            compiler_params=pltpu.CompilerParams(collective_id=0, has_side_effects=True),
            name="experts",
        )(tokens, norm_gain.reshape(1, half), routing, route_weight, w_gate, w_up, w_down)

    in_specs = (
        P("ep", "tp"), P("tp"), P("ep", None), P("ep", None),
        P("ep", None, "tp"), P("ep", None, "tp"), P("ep", None, "tp"),
    )
    return jax.shard_map(local, mesh=mesh, in_specs=in_specs, out_specs=P("ep", "tp"), check_vma=False)
```

time: 51.7 us -> 26.8 us (0.52)
  blocking collectives: 28.9 us -> 0 us
  Pallas kernels: 0 us -> 23 us
  waiting for transfers between devices: 10 us -> 0 us
  starting transfers between devices: 4.44 us -> 0 us
  other arithmetic: 2.39 us -> 0 us
  matrix products: 1.4 us -> 0 us
    pallas_call x0 -> x1, Pallas kernels: none -> 23 us  [local(): pl.pallas_call(functools.partial(kernel, n), out_shape=jax.ShapeDtypeStru...]
    all_to_all x1 -> x0, blocking collectives: 18.2 us -> none  [local(): lax.all_to_all(outgoing, 'ep', split_axis=0, concat_axis=0, tiled=True)]
    all_to_all x1 -> x0, waiting for transfers between devices: 10 us -> none  [local(): lax.all_to_all(for_sending(stacked), 'ep', split_axis=0, concat_axis=0, t...]
    all_gather x4 -> x0, blocking collectives: 8.05 us -> none  [taken_in(): lax.all_gather(part, axis, axis=dim, tiled=True)]
    all_to_all x1 -> x0, starting transfers between devices: 4.44 us -> none  [local(): lax.all_to_all(for_sending(stacked), 'ep', split_axis=0, concat_axis=0, t...]
    psum x1 -> x0, blocking collectives: 2.65 us -> none  [local(): total_squares = lax.psum(square_sum, 'tp')]
    unnamed x16 -> x7, local copies, waits for them, and re-layouts: 1.38 us -> 3.56 us
    dot_general x6 -> x0, matrix products: 1.4 us -> none  [the longest x2 0.48 us: add_feature(): jnp.dot(block_part, up_rows, preferred_element_type=jnp.float32)]
  transfers between devices with their start and end apart: 1 -> 0, of which waited for: 1 -> 0; matrix products, arithmetic and copies ran while one was open for 0% -> 0% of each run, Pallas kernels for 0% -> 0%
where the time goes in v1:
time: 26.8 us; the launch traced here: 26.6 us
  Pallas kernels  23 us (86%)
  local copies, waits for them, and re-layouts  3.56 us (13%)
    pallas_call x1, Pallas kernels, local(): pl.pallas_call(functools.partial(kernel, n), out_shape=jax.ShapeDtypeStru...  23 us
    unnamed x7, local copies, waits for them, and re-layouts  3.56 us

profile of v1, /device:TPU:0, one launch (start us, length us, event | category | flops | bytes accessed | tf_op | source)
XLA Modules:
  0.0 26.6 jit_solution(16426187810031837952)
XLA Ops:
  0.0 0.0 copy-start
  0.0 0.7 %copy-done = s32[64,2]{0,1:T(2,128)S(1)} copy-done((s32[64,2]{0,1:T(2,128)S(1)}, s32[64,2]{0,1:T(2,128)}, u32[]{:S(2)}) %copy-start) | copy-done | bytes 536
  0.7 0.0 copy-start.1
  0.7 0.7 %copy.8.routing_ref = s32[64,2]{1,0:T(8,128)} copy(s32[64,2]{0,1:T(2,128)S(1)} %copy-done) | data formatting | bytes 1024 | tf_op args[2]
  1.4 0.0 copy-done.1
  1.4 0.7 %copy.9.weight_ref = f32[64,2]{1,0:T(8,128)} copy(f32[64,2]{0,1:T(2,128)S(1)} %copy-done.1) | data formatting | bytes 1024 | tf_op args[3]
  2.1 23.0 %experts.1 = bf16[64,512]{1,0:T(8,128)(2,1)} custom-call(bf16[64,512]{1,0:T(8,128)(2,1)} %tok_ref.1, f32[1,512]{1,0:T(1,128)} %bitcast.1, s32[64,2]{1,0:T(8,128)} %copy.8.routing_ref, f32[64,2]{1,0:T(8,128)} %copy.9.weight_ref, bf16[2,1024,256]{2,1,0:T(8,128)(2,1)} %wg_hbm.1, bf16[2,1024,256]{2,1,0:T(8,128)(2,1)} %wu_hbm.1, bf16[2,512,512]{2,1,0:T(8,128)(2,1)} %wd_hbm.1), custom_call_target="tpu_custom_call" | custom-call | tf_op jit(solution)/shard_map/experts/pallas_call | solution.py:148
  25.1 1.5 %copy.11 = bf16[64,512]{1,0:T(8,128)(2,1)} copy(bf16[64,512]{1,0:T(8,128)(2,1)} %experts.1) | data formatting | bytes 131072
Async XLA Ops:
  0.0 0.7 %copy-start = (s32[64,2]{0,1:T(2,128)S(1)}, s32[64,2]{0,1:T(2,128)}, u32[]{:S(2)}) copy-start(s32[64,2]{0,1:T(2,128)} %param.9) | copy-start | bytes 1540
  0.7 0.7 %copy-start.1 = (f32[64,2]{0,1:T(2,128)S(1)}, f32[64,2]{0,1:T(2,128)}, u32[]{:S(2)}) copy-start(f32[64,2]{0,1:T(2,128)} %param.10) | copy-start | bytes 1540

commit v2 on v1

--- a/solution.py
+++ b/solution.py
@@ -21,21 +21,23 @@
 
 
 def kernel(
-    n, tok_ref, gain_ref, routing_ref, weight_ref, wg_hbm, wu_hbm, wd_hbm, out_ref,
-    gains, wg, wu, wd, send_x, recv_x, send_y, recv_y,
-    own_sem, far_send, far_recv, sx_sem, rx_sem, sy_sem, ry_sem,
+    n, tok_hbm, gain_hbm, routing_hbm, weight_hbm, wg_hbm, wu_hbm, wd_hbm, out_ref,
+    tok, routing, weight, gains, wg, wu, wd, send_x, recv_x, send_y, recv_y,
+    in_sem, own_sem, far_send, far_recv, sx_sem, rx_sem, sy_sem, ry_sem,
 ):
     me, core = lax.axis_index("ep"), lax.axis_index("tp")
     other = 1 - core
-    tokens, half = tok_ref.shape
+    tokens, half = tok.shape
     slots = 2 * n * CAP
 
     stores = ((wg_hbm, wg), (wu_hbm, wu), (wd_hbm, wd))
+    inputs = ((routing_hbm, routing), (tok_hbm, tok), (weight_hbm, weight), (gain_hbm, gains.at[core]))
+    inputs = [pltpu.make_async_copy(src, dst, in_sem.at[i]) for i, (src, dst) in enumerate(inputs)]
     own = [
         pltpu.make_async_copy(src.at[core], dst.at[core], own_sem.at[i])
         for i, (src, dst) in enumerate(stores)
     ]
-    for copy in own:
+    for copy in inputs:
         copy.start()
 
     barrier = pltpu.get_barrier_semaphore()
@@ -45,31 +47,34 @@
         for c in range(2):
             pl.semaphore_signal(barrier, inc=1, device_id=(peer, c), device_id_type=MESH)
 
+    each(n, greet)
     pl.semaphore_signal(barrier, inc=1, device_id=(me, other), device_id_type=MESH)
-    each(n, greet)
+    for copy in own:
+        copy.start()
 
-    gains[core] = gain_ref[...]
     experts = 2 * n
-    names = lax.broadcasted_iota(jnp.int32, (tokens, experts), 1)
-    picks = [routing_ref[:, k:k + 1] for k in range(2)]
-    hot = [(picks[k] == names).astype(jnp.float32) for k in range(2)]
+    names = lax.broadcasted_iota(jnp.int32, (experts, tokens), 0)
     row = lax.broadcasted_iota(jnp.int32, (tokens, tokens), 0)
     col = lax.broadcasted_iota(jnp.int32, (tokens, tokens), 1)
-    before = (col < row).astype(jnp.bfloat16)
-    earlier = jnp.dot(before, (hot[0] + hot[1]).astype(jnp.bfloat16), preferred_element_type=jnp.float32)
-    places = lax.broadcasted_iota(jnp.int32, (tokens, slots), 1)
+    before = (row < col).astype(jnp.float32).astype(jnp.bfloat16)
+    places = lax.broadcasted_iota(jnp.int32, (slots, tokens), 0)
+    inputs[0].wait()
+    picks = [routing[k:k + 1, :] for k in range(2)]
+    hot = [(picks[k] == names).astype(jnp.float32) for k in range(2)]
+    earlier = jnp.dot((hot[0] + hot[1]).astype(jnp.bfloat16), before, preferred_element_type=jnp.float32)
     chosen = []
     for k in range(2):
-        rank = jnp.sum(earlier * hot[k], axis=1, keepdims=True).astype(jnp.int32)
-        chosen.append(places == picks[k] * CAP + rank)
-    spread = (chosen[0] | chosen[1]).astype(jnp.float32).astype(jnp.bfloat16)
-    outgoing = lax.dot_general(
-        spread, tok_ref[...], (((0,), (0,)), ((), ())), preferred_element_type=jnp.float32
-    )
+        rank = jnp.sum(earlier * hot[k], axis=0, keepdims=True).astype(jnp.int32)
+        chosen.append((places == picks[k] * CAP + rank).astype(jnp.float32))
+    spread = (chosen[0] + chosen[1]).astype(jnp.bfloat16)
+    inputs[1].wait()
+    outgoing = jnp.dot(spread, tok[...], preferred_element_type=jnp.float32)
     send_x[...] = outgoing.reshape(2 * n, CAP, half).astype(jnp.bfloat16)
+    pick_rows = [jnp.transpose(c).astype(jnp.bfloat16) for c in chosen]
+    inputs[2].wait()
+    pick_weight = [jnp.transpose(jnp.broadcast_to(weight[k:k + 1, :], (CAP, tokens)))[:, :1] for k in range(2)]
 
     pl.semaphore_wait(barrier, 2 * n - 1)
-
     def remote(src, dst, send, recv, peer, c):
         return pltpu.make_async_remote_copy(
             src_ref=src, dst_ref=dst, send_sem=send, recv_sem=recv,
@@ -84,7 +89,8 @@
     each(n, post)
     remote(send_x.at[me * 2 + other], recv_x.at[core * n + me], sx_sem, rx_sem, me, other).start()
     pltpu.make_async_copy(send_x.at[me * 2 + core], recv_x.at[core * n + me], rx_sem).start()
-    far = [remote(gain_ref, gains.at[core], far_send.at[3], far_recv.at[3], me, other)] + [
+    inputs[3].wait()
+    far = [remote(gain_hbm, gains.at[core], far_send.at[3], far_recv.at[3], me, other)] + [
         remote(src.at[other], dst.at[core], far_send.at[i], far_recv.at[i], me, other)
         for i, (src, dst) in enumerate(stores)
     ]
@@ -96,7 +102,7 @@
     for copy in far:
         copy.wait()
     pltpu.make_async_copy(recv_x, recv_x, rx_sem).wait()
-
+    sent = pl.ds(0, 2 * n - 1)
     rows = n * CAP
     parts = [recv_x[h * n:(h + 1) * n].astype(jnp.float32).reshape(rows, half) for h in range(2)]
     squares = sum(jnp.sum(p * p, axis=1, keepdims=True) for p in parts)
@@ -113,7 +119,6 @@
     for f in range(2):
         result = jnp.dot(hidden, wd[f], preferred_element_type=jnp.float32)
         send_y[f * n:(f + 1) * n] = result.reshape(n, CAP, half).astype(jnp.bfloat16)
-
     def reply(k):
         peer = lax.rem(me + k, n)
         for c in range(2):
@@ -127,10 +132,8 @@
     back = recv_y[...].astype(jnp.float32).reshape(slots, half).astype(jnp.bfloat16)
     total = 0.0
     for k in range(2):
-        pick = chosen[k].astype(jnp.float32).astype(jnp.bfloat16)
-        total = total + weight_ref[:, k:k + 1] * jnp.dot(pick, back, preferred_element_type=jnp.float32)
+        total = total + pick_weight[k] * jnp.dot(pick_rows[k], back, preferred_element_type=jnp.float32)
     out_ref[...] = total.astype(jnp.bfloat16)
-    sent = pl.ds(0, 2 * n - 1)
     pltpu.make_async_copy(send_x.at[sent], send_x.at[sent], sx_sem).wait()
     pltpu.make_async_copy(send_y.at[sent], send_y.at[sent], sy_sem).wait()
 
@@ -147,20 +150,23 @@
         dma = pltpu.SemaphoreType.DMA
         return pl.pallas_call(
             functools.partial(kernel, n),
-            out_shape=jax.ShapeDtypeStruct((rows, half), jnp.bfloat16),
-            in_specs=[vmem] * 4 + [far] * 3,
+            out_shape=pltpu.VMEM((rows, half), jnp.bfloat16),
+            in_specs=[far] * 7,
             out_specs=vmem,
             scratch_shapes=[
+                pltpu.VMEM((rows, half), jnp.bfloat16),
+                pltpu.VMEM((2, rows), jnp.int32),
+                pltpu.VMEM((2, rows), jnp.float32),
                 pltpu.VMEM((2, 1, half), jnp.float32),
                 pltpu.VMEM(w_gate.shape, jnp.bfloat16),
                 pltpu.VMEM(w_up.shape, jnp.bfloat16),
                 pltpu.VMEM(w_down.shape, jnp.bfloat16),
                 blocks, blocks, blocks, blocks,
-                dma((3,)), dma((4,)), dma((4,)), dma, dma, dma, dma,
+                dma((4,)), dma((3,)), dma((4,)), dma((4,)), dma, dma, dma, dma,
             ],
             compiler_params=pltpu.CompilerParams(collective_id=0, has_side_effects=True),
             name="experts",
-        )(tokens, norm_gain.reshape(1, half), routing, route_weight, w_gate, w_up, w_down)
+        )(tokens, norm_gain.reshape(1, half), routing.T, route_weight.T, w_gate, w_up, w_down)
 
     in_specs = (
         P("ep", "tp"), P("tp"), P("ep", None), P("ep", None),

time: 26.8 us -> 22.4 us (0.84)
  local copies, waits for them, and re-layouts: 3.56 us -> 0.63 us
  Pallas kernels: 23 us -> 21.6 us
    unnamed x7 -> x1, local copies, waits for them, and re-layouts: 3.56 us -> 0.63 us
    pallas_call x1, Pallas kernels: 23 us -> 21.6 us  [local(): pl.pallas_call(functools.partial(kernel, n), out_shape=pltpu.VMEM((rows,...]
where the time goes in v2:
time: 22.4 us; the launch traced here: 22.2 us
  Pallas kernels  21.6 us (96%)
  local copies, waits for them, and re-layouts  0.63 us (3%)
    pallas_call x1, Pallas kernels, local(): pl.pallas_call(functools.partial(kernel, n), out_shape=pltpu.VMEM((rows,...  21.6 us
    unnamed x1, local copies, waits for them, and re-layouts  0.63 us

profile of v2, /device:TPU:0, one launch (start us, length us, event | category | flops | bytes accessed | tf_op | source)
XLA Modules:
  0.0 22.2 jit_solution(17427731982269932930)
XLA Ops:
  0.0 21.6 %experts.1 = bf16[64,512]{1,0:T(8,128)(2,1)S(1)} custom-call(bf16[64,512]{1,0:T(8,128)(2,1)} %tok_hbm.1, f32[1,512]{1,0:T(1,128)} %bitcast.3, s32[2,64]{1,0:T(2,128)} %bitcast.4, f32[2,64]{1,0:T(2,128)} %bitcast.5, bf16[2,1024,256]{2,1,0:T(8,128)(2,1)} %wg_hbm.1, bf16[2,1024,256]{2,1,0:T(8,128)(2,1)} %wu_hbm.1, bf16[2,512,512]{2,1,0:T(8,128)(2,1)} %wd_hbm.1), custom_call_target="tpu_custom_call" | custom-call | tf_op jit(solution)/shard_map/experts/pallas_call | solution.py:151
  21.6 0.6 %copy.9 = bf16[64,512]{1,0:T(8,128)(2,1)} copy(bf16[64,512]{1,0:T(8,128)(2,1)S(1)} %experts.1) | data formatting | bytes 131072

commit v3 on v2

v3 whole, which is shorter than its diff:
```python
import functools

import jax
import jax.numpy as jnp
from jax import lax
from jax.experimental import pallas as pl
from jax.experimental.pallas import tpu as pltpu
from jax.sharding import PartitionSpec as P

CAP = 8
EPSILON = 1e-06
MESH = pl.DeviceIdType.MESH


GROUPS = 4


def each(count, body):
    if count <= 16:
        for j in range(1, count):
            body(j)
    else:
        lax.fori_loop(1, count, lambda j, c: (body(j), c)[1], 0)


def ahead(me, j, n):
    return lax.rem(me + n - j, n)


def behind(me, j, n):
    return lax.rem(me + j, n)


def kernel(
    n, tok_hbm, gain_hbm, routing_hbm, weight_hbm, wg_hbm, wu_hbm, wd_hbm, out_ref,
    tok, routing, weight, gains, wg, wu, wd, give_g, give_u, give_d, send_x, recv_x, send_y, recv_y,
    in_sem, own_sem, give_sem, far_send, far_recv, sx_sem, rx_sem, sy_sem, ry_sem,
):
    me, core = lax.axis_index("ep"), lax.axis_index("tp")
    other = 1 - core
    tokens, half = tok.shape
    slots = 2 * n * CAP
    span = n // GROUPS

    stores = ((wg_hbm, wg, give_g), (wu_hbm, wu, give_u), (wd_hbm, wd, give_d))
    inputs = ((routing_hbm, routing), (tok_hbm, tok), (weight_hbm, weight), (gain_hbm, gains.at[core]))
    inputs = [pltpu.make_async_copy(src, dst, in_sem.at[i]) for i, (src, dst) in enumerate(inputs)]
    own = [
        pltpu.make_async_copy(src.at[core], dst.at[core], own_sem.at[i])
        for i, (src, dst, _) in enumerate(stores)
    ]
    give = [
        pltpu.make_async_copy(src.at[other], stage, give_sem.at[i])
        for i, (src, _, stage) in enumerate(stores)
    ]
    for copy in inputs:
        copy.start()

    barrier = pltpu.get_barrier_semaphore()

    def greet(j):
        peer = ahead(me, j, n)
        for c in range(2):
            pl.semaphore_signal(barrier, inc=1, device_id=(peer, c), device_id_type=MESH)

    each(n, greet)
    pl.semaphore_signal(barrier, inc=1, device_id=(me, other), device_id_type=MESH)
    for copy in give + own:
        copy.start()

    experts = 2 * n
    names = lax.broadcasted_iota(jnp.int32, (experts, tokens), 0)
    row = lax.broadcasted_iota(jnp.int32, (tokens, tokens), 0)
    col = lax.broadcasted_iota(jnp.int32, (tokens, tokens), 1)
    before = (row < col).astype(jnp.float32).astype(jnp.bfloat16)
    places = lax.broadcasted_iota(jnp.int32, (slots, tokens), 0)
    inputs[0].wait()
    picks = [routing[k:k + 1, :] for k in range(2)]
    hot = [(picks[k] == names).astype(jnp.float32) for k in range(2)]
    earlier = jnp.dot((hot[0] + hot[1]).astype(jnp.bfloat16), before, preferred_element_type=jnp.float32)
    chosen = []
    for k in range(2):
        rank = jnp.sum(earlier * hot[k], axis=0, keepdims=True).astype(jnp.int32)
        chosen.append((places == picks[k] * CAP + rank).astype(jnp.float32))
    spread = (chosen[0] + chosen[1]).astype(jnp.bfloat16)
    inputs[1].wait()
    outgoing = jnp.dot(spread, tok[...], preferred_element_type=jnp.float32)
    send_x[...] = outgoing.reshape(2 * n, CAP, half).astype(jnp.bfloat16)
    pick_rows = [jnp.transpose(c).astype(jnp.bfloat16) for c in chosen]
    inputs[2].wait()
    pick_weight = [jnp.transpose(jnp.broadcast_to(weight[k:k + 1, :], (CAP, tokens)))[:, :1] for k in range(2)]
    for copy in inputs[3:] + give:
        copy.wait()

    pl.semaphore_wait(barrier, 2 * n - 1)

    def remote(src, dst, send, recv, peer, c):
        return pltpu.make_async_remote_copy(
            src_ref=src, dst_ref=dst, send_sem=send, recv_sem=recv,
            device_id=(peer, c), device_id_type=MESH,
        )

    def block(j, h):
        return (j // span * 2 + h) * span + j % span

    gain_copy = remote(gains.at[core], gains.at[core], far_send.at[3], far_recv.at[3], me, other)
    gain_copy.start()
    remote(send_x.at[me * 2 + other], recv_x.at[block(0, core)], sx_sem, rx_sem.at[0], me, other).start()
    pltpu.make_async_copy(send_x.at[me * 2 + core], recv_x.at[block(0, core)], rx_sem.at[0]).start()

    def post(j):
        peer = ahead(me, j, n)
        for c in range(2):
            remote(
                send_x.at[peer * 2 + c], recv_x.at[block(j, core)], sx_sem, rx_sem.at[j // span], peer, c
            ).start()

    far = [
        remote(stage, dst.at[core], far_send.at[i], far_recv.at[i], me, other)
        for i, (_, dst, stage) in enumerate(stores)
    ]
    for copy in far:
        copy.start()
    each(n, post)

    for copy in own:
        copy.wait()
    gain_copy.wait()

    def reply(j):
        peer = behind(me, j, n)
        for c in range(2):
            remote(send_y.at[block(j, c)], recv_y.at[me * 2 + core], sy_sem, ry_sem, peer, c).start()

    rows = span * CAP
    for g in range(GROUPS):
        here = recv_x.at[pl.ds(2 * g * span, 2 * span)]
        pltpu.make_async_copy(here, here, rx_sem.at[g]).wait()
        parts = [
            recv_x[(2 * g + h) * span:(2 * g + h + 1) * span].astype(jnp.float32).reshape(rows, half)
            for h in range(2)
        ]
        squares = sum(jnp.sum(p * p, axis=1, keepdims=True) for p in parts)
        scale = lax.rsqrt(squares / (2 * half) + EPSILON)
        normed = jnp.concatenate(
            [(p * scale * gains[h]).astype(jnp.bfloat16) for h, p in enumerate(parts)], axis=1
        )
        if g == 0:
            far[0].wait()
            far[1].wait()
        hidden = []
        for h in range(2):
            gate = jnp.dot(normed, wg[h], preferred_element_type=jnp.float32)
            up = jnp.dot(normed, wu[h], preferred_element_type=jnp.float32)
            hidden.append((jax.nn.silu(gate) * up).astype(jnp.bfloat16))
        hidden = jnp.concatenate(hidden, axis=1)
        if g == 0:
            far[2].wait()
        for f in range(2):
            result = jnp.dot(hidden, wd[f], preferred_element_type=jnp.float32)
            first = (2 * g + f) * span
            send_y[first:first + span] = result.reshape(span, CAP, half).astype(jnp.bfloat16)
        if g == 0:
            remote(send_y.at[block(0, other)], recv_y.at[me * 2 + core], sy_sem, ry_sem, me, other).start()
            pltpu.make_async_copy(send_y.at[block(0, core)], recv_y.at[me * 2 + core], ry_sem).start()
        if span <= 16:
            for j in range(max(g * span, 1), (g + 1) * span):
                reply(j)
        else:
            lax.fori_loop(max(g * span, 1), (g + 1) * span, lambda j, c: (reply(j), c)[1], 0)

    pltpu.make_async_copy(recv_y, recv_y, ry_sem).wait()
    back = recv_y[...].astype(jnp.float32).reshape(slots, half).astype(jnp.bfloat16)
    total = 0.0
    for k in range(2):
        total = total + pick_weight[k] * jnp.dot(pick_rows[k], back, preferred_element_type=jnp.float32)
    out_ref[...] = total.astype(jnp.bfloat16)
    sent = pl.ds(0, 2 * n - 1)
    pltpu.make_async_copy(send_x.at[sent], send_x.at[sent], sx_sem).wait()
    pltpu.make_async_copy(send_y.at[sent], send_y.at[sent], sy_sem).wait()


def solution(mesh):
    n = mesh.shape["ep"]

    def local(tokens, norm_gain, routing, route_weight, w_gate, w_up, w_down):
        rows, half = tokens.shape
        assert w_gate.shape[0] == 2 and mesh.shape["tp"] == 2
        vmem = pl.BlockSpec(memory_space=pltpu.VMEM)
        far = pl.BlockSpec(memory_space=pl.ANY)
        blocks = pltpu.VMEM((2 * n, CAP, half), jnp.bfloat16)
        dma = pltpu.SemaphoreType.DMA
        return pl.pallas_call(
            functools.partial(kernel, n),
            out_shape=pltpu.VMEM((rows, half), jnp.bfloat16),
            in_specs=[far] * 7,
            out_specs=vmem,
            scratch_shapes=[
                pltpu.VMEM((rows, half), jnp.bfloat16),
                pltpu.VMEM((2, rows), jnp.int32),
                pltpu.VMEM((2, rows), jnp.float32),
                pltpu.VMEM((2, 1, half), jnp.float32),
                pltpu.VMEM(w_gate.shape, jnp.bfloat16),
                pltpu.VMEM(w_up.shape, jnp.bfloat16),
                pltpu.VMEM(w_down.shape, jnp.bfloat16),
                pltpu.VMEM(w_gate.shape[1:], jnp.bfloat16),
                pltpu.VMEM(w_up.shape[1:], jnp.bfloat16),
                pltpu.VMEM(w_down.shape[1:], jnp.bfloat16),
                blocks, blocks, blocks, blocks,
                dma((4,)), dma((3,)), dma((3,)), dma((4,)), dma((4,)), dma, dma((GROUPS,)), dma, dma,
            ],
            compiler_params=pltpu.CompilerParams(collective_id=0, has_side_effects=True),
            name="experts",
        )(tokens, norm_gain.reshape(1, half), routing.T, route_weight.T, w_gate, w_up, w_down)

    in_specs = (
        P("ep", "tp"), P("tp"), P("ep", None), P("ep", None),
        P("ep", None, "tp"), P("ep", None, "tp"), P("ep", None, "tp"),
    )
    return jax.shard_map(local, mesh=mesh, in_specs=in_specs, out_specs=P("ep", "tp"), check_vma=False)
```

time: 22.4 us -> 21.1 us (0.942)
  the two profiles are of different devices: /device:TPU:0 before, /device:TPU:13 now
where the time goes in v3:
time: 21.1 us; the launch traced here: 21 us
  Pallas kernels  20.3 us (96%)
  local copies, waits for them, and re-layouts  0.63 us (3%)
    pallas_call x1, Pallas kernels, local(): pl.pallas_call(functools.partial(kernel, n), out_shape=pltpu.VMEM((rows,...  20.3 us
    unnamed x1, local copies, waits for them, and re-layouts  0.63 us

profile of v3, /device:TPU:13, one launch (start us, length us, event | category | flops | bytes accessed | tf_op | source)
XLA Modules:
  0.0 21.0 jit_solution(3276476103440975206)
XLA Ops:
  0.0 20.3 %experts.1 = bf16[64,512]{1,0:T(8,128)(2,1)S(1)} custom-call(bf16[64,512]{1,0:T(8,128)(2,1)} %tok_hbm.1, f32[1,512]{1,0:T(1,128)} %bitcast.3, s32[2,64]{1,0:T(2,128)} %bitcast.4, f32[2,64]{1,0:T(2,128)} %bitcast.5, bf16[2,1024,256]{2,1,0:T(8,128)(2,1)} %wg_hbm.1, bf16[2,1024,256]{2,1,0:T(8,128)(2,1)} %wu_hbm.1, bf16[2,512,512]{2,1,0:T(8,128)(2,1)} %wd_hbm.1), custom_call_target="tpu_custom_call" | custom-call | tf_op jit(solution)/shard_map/experts/pallas_call | solution.py:193
  20.3 0.6 %copy.9 = bf16[64,512]{1,0:T(8,128)(2,1)} copy(bf16[64,512]{1,0:T(8,128)(2,1)S(1)} %experts.1) | data formatting | bytes 131072
